TPU v7x, 32 devices: a whole 2x2x4 slice. The times are simulated.
32 devices in a mesh: sp: 16 (over z, y, core), tp: 2 (over x).
Axes of the slice: x: 2, y: 2, z: 4, core: 2. Of those that a mesh axis runs over, the one named last changes fastest.
Arguments:
- queries: bfloat16 [3072, 1024], P('sp', 'tp'), may hold values from -6 to 6
- keys: bfloat16 [3072, 512], P('sp', 'tp'), may hold values from -6 to 6
- values: bfloat16 [3072, 512], P('sp', 'tp'), may hold values from -6 to 6
- q_gain: float32 [64], replicated, may hold values from 0.1 to 6.5
- k_gain: float32 [64], replicated, may hold values from 0.1 to 6.5
- w_out: bfloat16 [1024, 2048], P('tp'), may hold values from -12 to 12
- residual: bfloat16 [3072, 2048], P(('sp', 'tp')), may hold values from -6 to 6
- norm_gain: float32 [2048], replicated, may hold values from 0.1 to 1.9
- w_gate: bfloat16 [2048, 5632], P('sp', 'tp'), may hold values from -0.125 to 0.125
- w_up: bfloat16 [2048, 5632], P('sp', 'tp'), may hold values from -0.125 to 0.125
- w_down: bfloat16 [5632, 2048], P('tp', 'sp'), may hold values from -0.25 to 0.25
Outputs:
- layer_out: bfloat16 [3072, 2048], P(('sp', 'tp'))
All inputs are finite; a program needn't handle non-finite values.
Results may differ from a plain program's by a relative error of at most 0.018.
The roundings to bfloat16 on the way count: a program that leaves them out, or rounds other values in their place, can miss the bound.
Values may be sent and summed in bfloat16 or wider, within the bound.
A program may use at most 128 MiB of HBM per device.

v0:
```python
import math

import jax
import jax.numpy as jnp
from jax import lax
from jax.sharding import PartitionSpec as P

GRID_W = 128


EPS = 1e-06
THETA = 10000.0


def turn_half(part, angle):
    quarter = part.shape[-1] // 2
    cos_table = jnp.cos(angle)[:, None, :]
    sin_table = jnp.sin(angle)[:, None, :]
    first_part = part[..., :quarter]
    second_part = part[..., quarter:]
    return jnp.concatenate(
        [
            first_part * cos_table - second_part * sin_table,
            first_part * sin_table + second_part * cos_table,
        ],
        axis=-1,
    )


def head_norm_rope(flat, gain, offset, head_count):
    tok_rows = flat.shape[0]
    head_size = flat.shape[1] // head_count
    heads = flat.astype(jnp.float32).reshape(tok_rows, head_count, head_size)
    heads = heads * lax.rsqrt(jnp.mean(heads * heads, axis=-1, keepdims=True) + EPS) * gain
    positions = offset + jnp.arange(tok_rows, dtype=jnp.int32)
    row_pos = (positions // GRID_W).astype(jnp.float32)
    col_pos = (positions % GRID_W).astype(jnp.float32)
    half_size = head_size // 2
    inv_freq = THETA ** (-jnp.arange(0, half_size, 2, dtype=jnp.float32) / half_size)
    turned = jnp.concatenate(
        [
            turn_half(heads[..., :half_size], row_pos[:, None] * inv_freq[None, :]),
            turn_half(heads[..., half_size:], col_pos[:, None] * inv_freq[None, :]),
        ],
        axis=-1,
    )
    return turned.reshape(tok_rows, head_count * head_size).astype(jnp.bfloat16)


def body(queries, keys, values, q_gain, k_gain, w_out, residual, norm_gain, w_gate, w_up, w_down):
    tok_rows = queries.shape[0]
    head_size = q_gain.shape[0]
    q_heads = queries.shape[1] // head_size
    kv_heads = keys.shape[1] // head_size
    q_group = q_heads // kv_heads
    offset = lax.axis_index("sp") * tok_rows
    q_rot = head_norm_rope(queries, q_gain, offset, q_heads)
    k_rot = head_norm_rope(keys, k_gain, offset, kv_heads)
    query_groups = q_rot.reshape(tok_rows, kv_heads, q_group, head_size)
    score_scale = head_size ** (-0.5)
    start_state = (
        jnp.full((kv_heads, q_group, tok_rows), -1e30, jnp.float32),
        jnp.zeros((kv_heads, q_group, tok_rows), jnp.float32),
        jnp.zeros((kv_heads, q_group, tok_rows, head_size), jnp.float32),
    )
    running = start_state
    key_piece = lax.all_gather(k_rot, "sp", axis=0, tiled=True)
    value_piece = lax.all_gather(values, "sp", axis=0, tiled=True)
    piece_len = key_piece.shape[0]
    block_len = math.gcd(piece_len, 512)
    blocks = piece_len // block_len
    key_blocks = key_piece.reshape(blocks, block_len, kv_heads, head_size)
    value_blocks = value_piece.reshape(blocks, block_len, kv_heads, head_size)

    def update(state, block_pair):
        prior_max, totals, accum = state
        key_block, value_block = block_pair
        scores = (
            jnp.einsum(
                "qhgd,khd->hgqk", query_groups, key_block, preferred_element_type=jnp.float32
            )
            * score_scale
        )
        new_max = jnp.maximum(prior_max, jnp.max(scores, axis=-1))
        weights = jnp.exp(scores - new_max[..., None])
        factor = jnp.exp(prior_max - new_max)
        totals = totals * factor + jnp.sum(weights, axis=-1)
        accum = accum * factor[..., None] + jnp.einsum(
            "hgqk,khd->hgqd",
            weights.astype(jnp.bfloat16),
            value_block,
            preferred_element_type=jnp.float32,
        )
        return ((new_max, totals, accum), None)

    running, unused = lax.scan(update, running, (key_blocks, value_blocks))
    final_max, totals, accum = running
    mixed = accum / totals[..., None]
    attn = (
        jnp.transpose(mixed, (2, 0, 1, 3))
        .reshape(tok_rows, q_heads * head_size)
        .astype(jnp.bfloat16)
    )
    own_rows = lax.all_to_all(attn, "tp", split_axis=0, concat_axis=1, tiled=True)
    columns = own_rows
    proj = jnp.dot(
        columns, lax.all_gather(w_out, "tp", axis=0, tiled=True), preferred_element_type=jnp.float32
    )
    mid = residual.astype(jnp.float32) + proj
    normed = (
        mid * lax.rsqrt(jnp.mean(mid * mid, axis=-1, keepdims=True) + EPS) * norm_gain
    ).astype(jnp.bfloat16)
    gathered = lax.all_gather(normed, "tp", axis=0, tiled=True)
    columns = gathered
    gate = jnp.dot(
        columns,
        lax.all_gather(w_gate, "sp", axis=0, tiled=True),
        preferred_element_type=jnp.float32,
    )
    up_part = jnp.dot(
        columns, lax.all_gather(w_up, "sp", axis=0, tiled=True), preferred_element_type=jnp.float32
    )
    hidden = (jax.nn.silu(gate) * up_part).astype(jnp.bfloat16)
    terms = jnp.dot(
        hidden, lax.all_gather(w_down, "sp", axis=1, tiled=True), preferred_element_type=jnp.float32
    )
    down = lax.psum_scatter(
        terms.astype(jnp.bfloat16), "tp", scatter_dimension=0, tiled=True
    ).astype(jnp.float32)
    return (mid + 0.5 * down).astype(jnp.bfloat16)


def solution(mesh):
    return jax.shard_map(
        body,
        mesh=mesh,
        in_specs=(
            P("sp", "tp"),
            P("sp", "tp"),
            P("sp", "tp"),
            P(),
            P(),
            P("tp", None),
            P(("sp", "tp"), None),
            P(),
            P("sp", "tp"),
            P("sp", "tp"),
            P("tp", "sp"),
        ),
        out_specs=P(("sp", "tp"), None),
        check_vma=False,
    )
```

profile of v0, /device:TPU:1, one launch (start us, length us, event | category | flops | bytes accessed | tf_op | source)
XLA Modules:
  0.0 477.0 jit_solution(934830852998414411)
XLA Ops:
  6.6 1.0 copy.23
  7.7 0.7 fusion.24
  8.7 0.7 copy.24
  9.5 0.7 all-gather.9.cloned.1.call-update
  10.3 0.7 all-gather.11.cloned.1.call-update
  13.3 38.4 %all-gather.7.cloned.1.call-done = bf16[3072,256]{1,0:T(8,128)(2,1)} async-done(((bf16[192,256]{1,0:T(8,128)(2,1)}), bf16[3072,256]{1,0:T(8,128)(2,1)}) %all-gather.7.cloned.1.call-update) | async-done | bytes 1572880 | tf_op jit(solution)/shard_map/all_gather | solution.py:67
  51.7 4.6 reshape.207
  56.3 3.3 copy.28
  59.6 32.7 %all-gather.9.cloned.1.call-done = bf16[3072,256]{1,0:T(8,128)(2,1)} async-done(((bf16[192,256]{1,0:T(8,128)(2,1)}), bf16[3072,256]{1,0:T(8,128)(2,1)}) %all-gather.9.cloned.1.call-update) | async-done | bytes 1572880 | tf_op jit(solution)/shard_map/all_gather | solution.py:68
  92.3 4.6 reshape.208
  96.9 3.3 copy.29
  100.3 32.2 %while.15 = (s32[]{:T(128)}, f32[4,2,192]{2,1,0:T(2,128)S(1)}, f32[4,2,192]{2,1,0:T(2,128)S(1)}, f32[4,2,192,64]{2,3,1,0:T(8,128)}, bf16[6,512,4,64]{1,3,2,0:T(8...) while((s32[]{:T(128)}, f32[4,2,192]{2,1,0:T(2,128)S(1)}, ...), condition=%wide.region_5.6_spmd.clone, body=%wide.region_2.5_spmd.clone.sunk | while | flops 207920640 | bytes 14189729 | solution.py:96
  100.3 1.7 bitcast_reduce_fusion.2
  102.0 0.9 fusion.50
  103.1 1.8 fusion.52
  104.9 0.8 copy-done.1
  105.7 1.7 bitcast_reduce_fusion.2
  107.5 0.9 fusion.50
  108.5 1.8 fusion.52
  110.3 0.8 copy-done.1
  111.1 1.7 bitcast_reduce_fusion.2
  112.8 0.9 fusion.50
  113.8 1.8 fusion.52
  115.6 0.8 copy-done.1
  116.4 1.7 bitcast_reduce_fusion.2
  118.2 0.9 fusion.50
  119.2 1.8 fusion.52
  121.0 0.8 copy-done.1
  121.8 1.7 bitcast_reduce_fusion.2
  123.5 0.9 fusion.50
  124.5 1.8 fusion.52
  126.4 0.8 copy-done.1
  127.2 1.7 bitcast_reduce_fusion.2
  128.9 0.9 fusion.50
  129.9 1.8 fusion.52
  131.7 0.8 copy-done.1
  132.5 1.1 fusion.25
  134.0 9.5 %all_to_all.16 = bf16[2,96,512]{2,1,0:T(8,128)(2,1)S(1)} all-to-all(bf16[2,96,512]{2,1,0:T(8,128)(2,1)S(1)} %copy.30), channel_id=1, replica_groups=mesh['sp'=16,'tp'=2] {'tp'}, dimensions={0} | all-to-all | bytes 393216 | tf_op jit(solution)/shard_map/all_to_all | solution.py:104
  143.5 7.4 %all-gather.11.cloned.1.call-done = bf16[1024,2048]{1,0:T(8,128)(2,1)} async-done(((bf16[512,2048]{1,0:T(8,128)(2,1)}), bf16[1024,2048]{1,0:T(8,128)(2,1)}) %all-gather.11.cloned.1.call-update) | async-done | bytes 4194320 | tf_op jit(solution)/shard_map/all_gather | solution.py:107
  150.9 3.2 multiply_reduce_fusion
  154.3 10.8 %all_gather.24 = bf16[192,2048]{1,0:T(8,128)(2,1)S(1)} all-gather(bf16[96,2048]{1,0:T(8,128)(2,1)S(1)} %multiply_convert_fusion), channel_id=1, replica_groups=mesh['sp'=16,'tp'=2] {'tp'}, dimensions={0}, use_global_device_ids=true | all-gather | bytes 1179648 | tf_op jit(solution)/shard_map/all_gather | solution.py:113
  165.0 82.6 %all-gather.13.cloned.1.call-done = bf16[2048,2816]{1,0:T(8,128)(2,1)} async-done(((bf16[128,2816]{1,0:T(8,128)(2,1)}), bf16[2048,2816]{1,0:T(8,128)(2,1)}) %all-gather.13.cloned.1.call-update) | async-done | bytes 11534352 | tf_op jit(solution)/shard_map/all_gather | solution.py:117
  247.6 8.0 %fusion.30 = f32[192,2816]{1,0:T(8,128)} fusion(bf16[192,2048]{1,0:T(8,128)(2,1)S(1)} %all_gather.24, bf16[2048,2816]{1,0:T(8,128)(2,1)} %all-gather.13.cloned.1.call-done), kind=kOutput, calls=%fused_computation.69 | convolution fusion | flops 2214592512 | bytes 14483456 | tf_op jit(solution)/shard_map/dot_general | solution.py:115
  255.7 86.4 %all-gather.15.cloned.1.call-done = bf16[2048,2816]{1,0:T(8,128)(2,1)} async-done(((bf16[128,2816]{1,0:T(8,128)(2,1)}), bf16[2048,2816]{1,0:T(8,128)(2,1)}) %all-gather.15.cloned.1.call-update) | async-done | bytes 11534352 | tf_op jit(solution)/shard_map/all_gather | solution.py:121
  342.0 97.2 %all-gather.17.cloned.1.call-done = bf16[2816,2048]{1,0:T(8,128)(2,1)} async-done(((bf16[2816,128]{1,0:T(8,128)(2,1)}), bf16[2816,2048]{1,0:T(8,128)(2,1)}) %all-gather.17.cloned.1.call-update) | async-done | bytes 11534352 | tf_op jit(solution)/shard_map/all_gather | solution.py:125
  439.2 13.9 %convolution_convert_fusion = bf16[192,2048]{1,0:T(8,128)(2,1)} fusion(bf16[2816,2048]{1,0:T(8,128)(2,1)} %all-gather.17.cloned.1.call-done, bf16[192,2048]{1,0:T(8,128)(2,1)S(1)} %all_gather.24, bf16[2048,2816]{1,0:T(8,128)(2,1)} %all-gather.15.cloned.1.call-done, f32[192,2816]{1,0:T(8,128)} %fusion.30), kind=kOutput, calls=%fused_computation.25 | convolution fusion | flops 4432822272 | bytes 26804224 | tf_op jit(solution)/shard_map/dot_general | solution.py:124
  453.1 15.3 %reduce-scatter.2.cloned.1.call-done = bf16[96,2048]{1,0:T(8,128)(2,1)} async-done(((bf16[192,2048]{1,0:T(8,128)(2,1)}), bf16[96,2048]{1,0:T(8,128)(2,1)}) %reduce-scatter.2.cloned.1.call-update) | async-done | bytes 393232 | tf_op jit(solution)/shard_map/reduce_scatter | solution.py:127
  468.3 1.8 add_convert_fusion
  (75 shorter events, 3.8 us)
Async XLA Ops:
  6.5 6.3 %copy-start.2 = (bf16[192,512]{1,0:T(8,128)(2,1)S(1)}, bf16[192,512]{1,0:T(8,128)(2,1)}, u32[]{:S(2)}) copy-start(bf16[192,512]{1,0:T(8,128)(2,1)} %param.13) | copy-start | bytes 589828
  6.5 45.2 %all-gather.7.cloned.1.call-start = ((), (), s32[]{:S(2)}) async-start(), calls=%async_computation.2 | async-start | bytes 1671168 | tf_op jit(solution)/shard_map/all_gather | solution.py:67
  8.4 4.6 copy-start.4
  9.5 82.8 %all-gather.9.cloned.1.call-start = ((), (), s32[]{:S(2)}) async-start(), calls=%async_computation.3 | async-start | bytes 1671168 | tf_op jit(solution)/shard_map/all_gather | solution.py:68
  10.2 140.6 %all-gather.11.cloned.1.call-start = ((), (), s32[]{:S(2)}) async-start(), calls=%async_computation.4 | async-start | bytes 6291456 | tf_op jit(solution)/shard_map/all_gather | solution.py:107
  11.0 236.7 %all-gather.13.cloned.1.call-start = ((), (), s32[]{:S(2)}) async-start(), calls=%async_computation.5 | async-start | bytes 12255232 | tf_op jit(solution)/shard_map/all_gather | solution.py:117
  11.6 330.5 %all-gather.15.cloned.1.call-start = ((), (), s32[]{:S(2)}) async-start(), calls=%async_computation.6 | async-start | bytes 12255232 | tf_op jit(solution)/shard_map/all_gather | solution.py:121
  12.1 427.1 %all-gather.17.cloned.1.call-start = ((), (), s32[]{:S(2)}) async-start(), calls=%async_computation.7 | async-start | bytes 12255232 | tf_op jit(solution)/shard_map/all_gather | solution.py:125
  12.7 455.6 %reduce-scatter.2.cloned.1.call-start = ((), (), s32[]{:S(2)}) async-start(), calls=%async_computation.8 | async-start | bytes 1179648 | tf_op jit(solution)/shard_map/reduce_scatter | solution.py:127
  102.0 1.1 copy-start
  104.9 0.8 copy-start.1
  107.4 1.0 copy-start
  110.3 0.8 copy-start.1
  112.8 1.0 copy-start
  115.6 0.8 copy-start.1
  118.1 1.0 copy-start
  121.0 0.8 copy-start.1
  123.5 1.0 copy-start
  126.3 0.8 copy-start.1
  128.9 1.0 copy-start
  131.7 0.8 copy-start.1
  133.9 20.2 %copy-start.3 = (f32[2048]{0:T(1024)S(1)}, f32[2048]{0:T(1024)}, u32[]{:S(2)}) copy-start(f32[2048]{0:T(1024)} %param.20) | copy-start | bytes 24580
Sparse Core Ops, SparseCore 0:
  9.6 42.0 all-gather.6
  54.0 38.2 all-gather.8
  93.9 56.9 all-gather.10
  153.0 94.5 all-gather.12
  249.8 92.2 all-gather.14
  344.0 95.1 all-gather.16
  453.2 15.0 reduce-scatter.1
where the time goes:
time: 479 us; the launch traced here: 477 us
  waiting for transfers between devices  363 us (76%)
  matrix products  46 us (10%)
  local copies, waits for them, and re-layouts  23.4 us (5%)
  blocking collectives  20.3 us (4%)
  between operations  13.7 us (3%)
  other arithmetic  10.2 us (2%)
    all_gather x1, waiting for transfers between devices, body(): lax.all_gather(w_down, 'sp', axis=1, tiled=True)  97.2 us
    all_gather x1, waiting for transfers between devices, body(): lax.all_gather(w_up, 'sp', axis=0, tiled=True)  86.4 us
    all_gather x1, waiting for transfers between devices, body(): lax.all_gather(w_gate, 'sp', axis=0, tiled=True)  82.6 us
    all_gather x1, waiting for transfers between devices, body(): key_piece = lax.all_gather(k_rot, 'sp', axis=0, tiled=True)  38.4 us
    all_gather x1, waiting for transfers between devices, body(): value_piece = lax.all_gather(values, 'sp', axis=0, tiled=True)  32.7 us
    reduce_scatter x1, waiting for transfers between devices, body(): lax.psum_scatter(terms.astype(jnp.bfloat16), 'tp', scatter_dimension=0, t...  15.3 us
    dot_general x1, matrix products, body(): jnp.dot(hidden, lax.all_gather(w_down, 'sp', axis=1, tiled=True), preferr...  13.9 us
    dot_general x6, matrix products, update(): jnp.einsum('hgqk,khd->hgqd', weights.astype(jnp.bfloat16), value_block, p...  10.8 us
  transfers between devices with their start and end apart: 7, of which 7 were waited for; matrix products, arithmetic and copies ran while one was open for 12% of the time, Pallas kernels for 0%

commit v1 on v0

--- a/solution.py
+++ b/solution.py
@@ -1,8 +1,11 @@
+import functools
 import math
 
 import jax
 import jax.numpy as jnp
 from jax import lax
+from jax.experimental import pallas as pl
+from jax.experimental.pallas import tpu as pltpu
 from jax.sharding import PartitionSpec as P
 
 GRID_W = 128
@@ -130,9 +133,301 @@
     return (mid + 0.5 * down).astype(jnp.bfloat16)
 
 
+MESH = pl.DeviceIdType.MESH
+
+
+def physical_ring(mesh):
+    count = mesh.shape["sp"]
+    try:
+        places = [(tuple(d.coords), d.core_on_chip) for d in mesh.devices[:, 0].flat]
+    except AttributeError:
+        return None
+    if count % 4 or count < 12:
+        return None
+    first = places[0][0]
+    depth = count // 4
+    for at, (coords, core) in enumerate(places):
+        chip = at // 2
+        want = (first[0], first[1] + chip % 2, first[2] + chip // 2)
+        if coords != want or core != at % 2:
+            return None
+    return depth
+
+
+def rope_kernel(head_size, q_ref, k_ref, qg_ref, kg_ref, cos_ref, sin_ref, q_out, k_out):
+    def one(x_ref, g_ref, out_ref, scale):
+        x = x_ref[...].astype(jnp.float32)
+        width = x.shape[1]
+        lane = lax.broadcasted_iota(jnp.int32, (width, width), 0) // head_size
+        other = lax.broadcasted_iota(jnp.int32, (width, width), 1) // head_size
+        same = (lane == other).astype(jnp.float32)
+        mean = jnp.dot(
+            x * x, same, preferred_element_type=jnp.float32, precision=lax.Precision.HIGHEST
+        ) * (1.0 / head_size)
+        h = x * lax.rsqrt(mean + EPS) * g_ref[...]
+        quarter = head_size // 4
+        repeats = width // cos_ref.shape[1]
+        cos_table = jnp.concatenate([cos_ref[...]] * repeats, axis=1)
+        sin_table = jnp.concatenate([sin_ref[...]] * repeats, axis=1)
+        at = lax.broadcasted_iota(jnp.int32, x.shape, 1)
+        is_first = (at // quarter) % 2 == 0
+        ahead = pltpu.roll(h, width - quarter, 1)
+        behind = pltpu.roll(h, quarter, 1)
+        turned = h * cos_table + jnp.where(is_first, -ahead, behind) * sin_table
+        out_ref[...] = (turned.astype(jnp.bfloat16) * scale).astype(jnp.bfloat16)
+
+    one(q_ref, qg_ref, q_out, head_size ** (-0.5))
+    one(k_ref, kg_ref, k_out, 1.0)
+
+
+def gather_attend_kernel(
+    depth,
+    q_ref, kv_in, wg_in, wu_in, wd_in,
+    attn_ref, wg_out, wu_out, wd_out,
+    kv_all, own_sem, ring_send, ring_recv, sib_send, sib_recv,
+):
+    n = 2 * depth
+    sp = lax.axis_index("sp")
+    tp = lax.axis_index("tp")
+    core = sp % 2
+    z = sp // 4
+    y = (sp // 2) % 2
+    pos = (1 - y) * z + y * (n - 1 - z)
+
+    def at_pos(p, c):
+        p = lax.rem(p + n, n)
+        yy = p // depth
+        zz = (1 - yy) * p + yy * (n - 1 - p)
+        return (zz * 2 + yy) * 2 + c
+
+    sibling = (at_pos(pos, 1 - core), tp)
+    toward = ((at_pos(pos + 1, core), tp), (at_pos(pos - 1, core), tp))
+
+    barrier = pltpu.get_barrier_semaphore()
+    for target in (sibling,) + toward:
+        pl.semaphore_signal(barrier, inc=1, device_id=target, device_id_type=MESH)
+    pl.semaphore_wait(barrier, 3)
+
+    tok = kv_in.shape[0]
+    rows = wg_in.shape[0]
+
+    def half(size, way):
+        return pl.ds(way * (size // 2), size // 2)
+
+    def part(start, size, way):
+        return pl.ds(pl.multiple_of(start * size + way * (size // 2), size // 2), size // 2)
+
+    ins = (
+        lambda way: kv_in.at[half(tok, way), :],
+        lambda way: wg_in.at[half(rows, way), :],
+        lambda way: wu_in.at[half(rows, way), :],
+        lambda way: wd_in.at[half(wd_in.shape[0], way), :],
+    )
+    outs = (
+        lambda o, way: kv_all.at[part(o, tok, way), :],
+        lambda o, way: wg_out.at[part(o, rows, way), :],
+        lambda o, way: wu_out.at[part(o, rows, way), :],
+        lambda o, way: wd_out.at[o, half(wd_in.shape[0], way), :],
+    )
+    own_outs = (
+        kv_all.at[pl.ds(pl.multiple_of(sp * tok, tok), tok), :],
+        wg_out.at[pl.ds(pl.multiple_of(sp * rows, rows), rows), :],
+        wu_out.at[pl.ds(pl.multiple_of(sp * rows, rows), rows), :],
+        wd_out.at[sp],
+    )
+    own = [
+        pltpu.make_async_copy(src, dst, own_sem.at[i])
+        for i, (src, dst) in enumerate(zip((kv_in, wg_in, wu_in, wd_in), own_outs))
+    ]
+
+    def owner(step, way, c):
+        return at_pos(pos - step if way == 0 else pos + step, c)
+
+    def ring(kind, step, way):
+        o = owner(step, way, core)
+        src = ins[kind](way) if step == 0 else outs[kind](o, way)
+        return pltpu.make_async_remote_copy(
+            src_ref=src, dst_ref=outs[kind](o, way),
+            send_sem=ring_send.at[kind, step, way], recv_sem=ring_recv.at[kind, step, way],
+            device_id=toward[way], device_id_type=MESH,
+        )
+
+    def arrived(kind, step, way):
+        o = owner(step + 1, way, core)
+        pltpu.make_async_remote_copy(
+            src_ref=outs[kind](o, way), dst_ref=outs[kind](o, way),
+            send_sem=ring_send.at[kind, step, way], recv_sem=ring_recv.at[kind, step, way],
+            device_id=toward[way], device_id_type=MESH,
+        ).wait_recv()
+
+    def across(kind, step, way, c):
+        o = owner(step, way, c)
+        src = ins[kind](way) if step == 0 else outs[kind](o, way)
+        return pltpu.make_async_remote_copy(
+            src_ref=src, dst_ref=outs[kind](o, way),
+            send_sem=sib_send.at[kind, step, way], recv_sem=sib_recv.at[kind, step, way],
+            device_id=sibling, device_id_type=MESH,
+        )
+
+    def serve(kind, step):
+        for way in range(2):
+            if step > 0:
+                arrived(kind, step - 1, way)
+            if step < n - 1:
+                ring(kind, step, way).start()
+            across(kind, step, way, core).start()
+
+    def finish(kind):
+        for step in range(n):
+            for way in range(2):
+                if step < n - 1:
+                    ring(kind, step, way).wait_send()
+                across(kind, step, way, core).wait_send()
+                o = owner(step, way, 1 - core)
+                pltpu.make_async_remote_copy(
+                    src_ref=outs[kind](o, way), dst_ref=outs[kind](o, way),
+                    send_sem=sib_send.at[kind, step, way], recv_sem=sib_recv.at[kind, step, way],
+                    device_id=sibling, device_id_type=MESH,
+                ).wait_recv()
+
+    own[0].start()
+    for step in range(n):
+        serve(0, step)
+        if step == n - 2:
+            for kind in (1, 2, 3):
+                own[kind].start()
+    for kind in (1, 2, 3):
+        serve(kind, 0)
+    own[0].wait()
+    finish(0)
+
+    pairs, q_rows, lanes = q_ref.shape
+    block = math.gcd(q_rows, 256)
+    per_pair = q_rows // block
+
+    def attend(at):
+        pair, which = at // per_pair, at % per_pair
+        span = slice(which * block, (which + 1) * block)
+        q = q_ref[pair, span, :]
+        k = kv_all[:, pair * lanes:(pair + 1) * lanes]
+        v = kv_all[:, (pairs + pair) * lanes:(pairs + pair + 1) * lanes]
+        scores = lax.dot_general(
+            q, k, (((1,), (1,)), ((), ())), preferred_element_type=jnp.float32
+        )
+        weights = jnp.exp(scores - jnp.max(scores, axis=-1, keepdims=True))
+        total = jnp.sum(weights, axis=-1, keepdims=True)
+        mixed = jnp.dot(weights.astype(jnp.bfloat16), v, preferred_element_type=jnp.float32)
+        attn_ref[pair, span, :] = (mixed / total).astype(jnp.bfloat16)
+
+    todo = list(range(pairs * per_pair))
+    for step in range(1, n):
+        for kind in (1, 2, 3):
+            serve(kind, step)
+            if todo:
+                attend(todo.pop(0))
+    for at in todo:
+        attend(at)
+    for kind in (1, 2, 3):
+        own[kind].wait()
+        finish(kind)
+
+
+def fast_body(depth, queries, keys, values, q_gain, k_gain, w_out, residual, norm_gain, w_gate, w_up, w_down):
+    tok_rows = queries.shape[0]
+    head_size = q_gain.shape[0]
+    q_heads = queries.shape[1] // head_size
+    kv_heads = keys.shape[1] // head_size
+    q_group = q_heads // kv_heads
+    n_sp = 4 * depth
+    positions = lax.axis_index("sp") * tok_rows + jnp.arange(tok_rows, dtype=jnp.int32)
+    half_size = head_size // 2
+    inv_freq = THETA ** (-jnp.arange(0, half_size, 2, dtype=jnp.float32) / half_size)
+    row_angle = (positions // GRID_W).astype(jnp.float32)[:, None] * inv_freq[None, :]
+    col_angle = (positions % GRID_W).astype(jnp.float32)[:, None] * inv_freq[None, :]
+    angle = jnp.concatenate([row_angle, row_angle, col_angle, col_angle] * 2, axis=1)
+    cos_table, sin_table = jnp.cos(angle), jnp.sin(angle)
+    q_rot, k_rot = pl.pallas_call(
+        functools.partial(rope_kernel, head_size),
+        out_shape=(
+            jax.ShapeDtypeStruct(queries.shape, jnp.bfloat16),
+            jax.ShapeDtypeStruct(keys.shape, jnp.bfloat16),
+        ),
+        name="rope",
+    )(
+        queries, keys,
+        jnp.tile(q_gain, q_heads)[None, :], jnp.tile(k_gain, kv_heads)[None, :],
+        cos_table, sin_table,
+    )
+    pairs = kv_heads // 2
+    grouped = q_rot.reshape(tok_rows, pairs, 2, q_group, head_size)
+    grouped = jnp.transpose(grouped, (1, 2, 3, 0, 4))
+    empty = jnp.zeros_like(grouped[:, 0])
+    padded = jnp.stack(
+        [
+            jnp.concatenate([grouped[:, 0], empty], axis=-1),
+            jnp.concatenate([empty, grouped[:, 1]], axis=-1),
+        ],
+        axis=1,
+    ).reshape(pairs, 2 * q_group * tok_rows, 2 * head_size)
+    kv = jnp.concatenate([k_rot, values], axis=1)
+    tokens = n_sp * tok_rows
+    any_space = pl.BlockSpec(memory_space=pl.ANY)
+    vmem = pl.BlockSpec(memory_space=pltpu.VMEM)
+    n = 2 * depth
+    attn_pad, wg_all, wu_all, wd_all = pl.pallas_call(
+        functools.partial(gather_attend_kernel, depth),
+        out_shape=(
+            jax.ShapeDtypeStruct(padded.shape, jnp.bfloat16),
+            jax.ShapeDtypeStruct((n_sp * w_gate.shape[0], w_gate.shape[1]), jnp.bfloat16),
+            jax.ShapeDtypeStruct((n_sp * w_up.shape[0], w_up.shape[1]), jnp.bfloat16),
+            jax.ShapeDtypeStruct((n_sp,) + w_down.shape, jnp.bfloat16),
+        ),
+        in_specs=[vmem, vmem, any_space, any_space, any_space],
+        out_specs=(vmem, any_space, any_space, any_space),
+        scratch_shapes=[
+            pltpu.VMEM((tokens, kv.shape[1]), jnp.bfloat16),
+            pltpu.SemaphoreType.DMA((4,)),
+            pltpu.SemaphoreType.DMA((4, n - 1, 2)),
+            pltpu.SemaphoreType.DMA((4, n - 1, 2)),
+            pltpu.SemaphoreType.DMA((4, n, 2)),
+            pltpu.SemaphoreType.DMA((4, n, 2)),
+        ],
+        compiler_params=pltpu.CompilerParams(
+            collective_id=0, has_side_effects=True, vmem_limit_bytes=48 * 1024 * 1024
+        ),
+        cost_estimate=pl.CostEstimate(
+            flops=150_000_000_000, bytes_accessed=80_000_000, transcendentals=0
+        ),
+        name="gather_attend",
+    )(padded, kv, w_gate, w_up, w_down)
+    parts = attn_pad.reshape(pairs, 2, q_group, tok_rows, 2, head_size)
+    attn = jnp.stack([parts[:, 0, :, :, 0], parts[:, 1, :, :, 1]], axis=1)
+    attn = jnp.transpose(attn, (3, 0, 1, 2, 4)).reshape(tok_rows, q_heads * head_size)
+    own_rows = lax.all_to_all(attn, "tp", split_axis=0, concat_axis=1, tiled=True)
+    proj = jnp.dot(
+        own_rows, lax.all_gather(w_out, "tp", axis=0, tiled=True), preferred_element_type=jnp.float32
+    )
+    mid = residual.astype(jnp.float32) + proj
+    normed = (
+        mid * lax.rsqrt(jnp.mean(mid * mid, axis=-1, keepdims=True) + EPS) * norm_gain
+    ).astype(jnp.bfloat16)
+    columns = lax.all_gather(normed, "tp", axis=0, tiled=True)
+    gate = jnp.dot(columns, wg_all, preferred_element_type=jnp.float32)
+    up_part = jnp.dot(columns, wu_all, preferred_element_type=jnp.float32)
+    hidden = (jax.nn.silu(gate) * up_part).astype(jnp.bfloat16)
+    terms = jnp.einsum("th,nho->tno", hidden, wd_all, preferred_element_type=jnp.float32)
+    terms = terms.reshape(tok_rows, -1)
+    down = lax.psum_scatter(
+        terms.astype(jnp.bfloat16), "tp", scatter_dimension=0, tiled=True
+    ).astype(jnp.float32)
+    return (mid + 0.5 * down).astype(jnp.bfloat16)
+
+
 def solution(mesh):
+    depth = physical_ring(mesh)
+    inner = body if depth is None else functools.partial(fast_body, depth)
     return jax.shard_map(
-        body,
+        inner,
         mesh=mesh,
         in_specs=(
             P("sp", "tp"),

time: 479 us -> 286 us (0.60)
  waiting for transfers between devices: 363 us -> 18.2 us
  Pallas kernels: 0 us -> 201 us
  matrix products: 46 us -> 24 us
  local copies, waits for them, and re-layouts: 23.4 us -> 8 us
  other arithmetic: 10.2 us -> 3.55 us
    all_gather x6 -> x1, waiting for transfers between devices: 345 us -> 0.02 us  [fast_body(): lax.all_gather(w_out, 'tp', axis=0, tiled=True)]
    pallas_call x0 -> x2, Pallas kernels: none -> 201 us  [the longest x1 198 us: fast_body(): pl.pallas_call(functools.partial(gather_attend_kernel, depth), out_shape=...]
    dot_general x15 -> x3, matrix products: 46 us -> 24 us  [the longest x1 12.9 us: fast_body(): jnp.einsum('th,nho->tno', hidden, wd_all, preferred_element_type=jnp.floa...]
    reshape x2 -> x1, local copies, waits for them, and re-layouts: 9.18 us -> 0.42 us  [fast_body(): parts = attn_pad.reshape(pairs, 2, q_group, tok_rows, 2, head_size)]
    unnamed x10 -> x12, local copies, waits for them, and re-layouts: 7.86 us -> 0.03 us
    reduce_sum x8 -> x0, other arithmetic: 5.67 us -> none  [the longest x6 5.55 us: update(): totals = totals * factor + jnp.sum(weights, axis=-1)]
    while x30 -> x0, local copies, waits for them, and re-layouts: 5.28 us -> none
  transfers between devices with their start and end apart: 7 -> 2, of which waited for: 7 -> 1; matrix products, arithmetic and copies ran while one was open for 12% -> 3% of each run, Pallas kernels for 0% -> 70%
where the time goes in v1:
time: 286 us; the launch traced here: 285 us
  Pallas kernels  201 us (70%)
  matrix products  24 us (8%)
  waiting for transfers between devices  18.2 us (6%)
  blocking collectives  16.8 us (6%)
  between operations  13.6 us (5%)
  local copies, waits for them, and re-layouts  8 us (3%)
  other arithmetic  3.55 us (1%)
    pallas_call x1, Pallas kernels, fast_body(): pl.pallas_call(functools.partial(gather_attend_kernel, depth), out_shape=...  198 us
    reduce_scatter x1, waiting for transfers between devices, fast_body(): lax.psum_scatter(terms.astype(jnp.bfloat16), 'tp', scatter_dimension=0, t...  17.4 us
    dot_general x1, matrix products, fast_body(): jnp.einsum('th,nho->tno', hidden, wd_all, preferred_element_type=jnp.floa...  12.9 us
    all_gather x1, blocking collectives, fast_body(): columns = lax.all_gather(normed, 'tp', axis=0, tiled=True)  10.1 us
    dot_general x1, matrix products, fast_body(): gate = jnp.dot(columns, wg_all, preferred_element_type=jnp.float32)  7.99 us
    all_to_all x1, blocking collectives, fast_body(): lax.all_to_all(attn, 'tp', split_axis=0, concat_axis=1, tiled=True)  6.69 us
  transfers between devices with their start and end apart: 2, of which 1 were waited for; matrix products, arithmetic and copies ran while one was open for 3% of the time, Pallas kernels for 70%

profile of v1, /device:TPU:1, one launch (start us, length us, event | category | flops | bytes accessed | tf_op | source)
XLA Modules:
  0.0 285.2 jit_solution(11176032067869270188)
XLA Ops:
  6.5 0.0 copy-start.4
  6.5 0.0 copy-start.2
  6.5 0.0 copy-start.1
  6.5 0.0 copy-start
  6.5 0.0 all-gather.2.cloned.1.call-start
  6.6 0.7 all-gather.2.cloned.1.call-update
  7.3 0.0 reduce-scatter.2.cloned.1.call-start
  7.4 0.7 tile.5
  8.0 0.7 broadcast_in_dim_tile.7.kg_ref
  8.7 0.7 tile.4
  9.3 0.7 broadcast_in_dim_tile.6.qg_ref
  10.0 0.1 broadcast_multiply_fusion
  10.1 0.3 concatenate.12
  10.4 1.0 fusion.7
  11.4 3.0 %rope.1 = (bf16[192,512]{1,0:T(8,128)(2,1)}, bf16[192,256]{1,0:T(8,128)(2,1)}) custom-call(bf16[192,512]{1,0:T(8,128)(2,1)} %q_ref.1, bf16[192,256]{1,0:T(8,128)(2,1)} %k_ref.1, f32[1,512]{1,0:T(1,128)} %broadcast_in_dim_tile.6.qg_ref, f32[1,256]{1,0:T(1,128)} %broadcast_in_dim_tile.7.kg_ref, f32[192,128]{1,0:T(8,128)} %get-tuple-element.22.cos_ref, ...), custom_call_target="tpu_custom_call" | custom-call | tf_op jit(solution)/shard_map/rope/pallas_call | solution.py:349
  14.4 1.1 copy.25
  15.5 0.1 pad_maximum_fusion
  15.6 0.3 copy.27
  15.9 0.0 copy-done.4
  15.9 0.9 pad_maximum_fusion.1.kv_in
  16.8 0.0 copy-done.2
  16.8 0.0 copy-done.1
  16.8 0.0 copy-done
  16.9 197.9 %gather_attend.1 = (bf16[2,768,128]{2,1,0:T(8,128)(2,1)S(1)}, bf16[2048,2816]{1,0:T(8,128)(2,1)}, bf16[2048,2816]{1,0:T(8,128)(2,1)}, bf16[16,2816,128]{2,1,0:T(8,128)(2,1)}) custom-call(bf16[2,768,128]{2,1,0:T(8,128)(2,1)S(1)} %bitcast.41, bf16[192,512]{1,0:T(8,128)(2,1)S(1)} %pad_maximum_fusion.1.kv_in, bf16[128,2816]{1,0:T(8,128)(2,1)S(1)} %copy-done, ...), custom_call_target="tpu_custom_call" | custom-call | flops 149999992832 | bytes 80000000 | tf_op jit(solution)/shard_map/gather_attend/pallas_call | solution.py:377
  214.8 0.0 copy-start.3
  214.8 0.2 copy.28
  215.0 0.4 reshape.70
  215.4 0.2 slice_bitcast_fusion.1
  215.6 0.0 copy-start.5
  215.6 0.4 maximum_bitcast_fusion
  216.1 0.5 copy.36
  216.6 0.3 reshape.72
  216.8 6.7 %all_to_all.19 = bf16[2,96,512]{2,1,0:T(8,128)(2,1)S(1)} all-to-all(bf16[2,96,512]{2,1,0:T(8,128)(2,1)S(1)} %reshape.72), channel_id=1, replica_groups=mesh['sp'=16,'tp'=2] {'tp'}, dimensions={0} | all-to-all | bytes 393216 | tf_op jit(solution)/shard_map/all_to_all | solution.py:406
  223.5 0.0 all-gather.2.cloned.1.call-done
  223.6 0.0 copy-done.3
  223.6 3.1 %multiply_reduce_fusion = (f32[96]{0:T(128)S(1)}, f32[96,2048]{1,0:T(8,128)S(1)}) fusion(bf16[96,1024]{1,0:T(8,128)(2,1)S(1)} %bitcast.44, bf16[1024,2048]{1,0:T(8,128)(2,1)} %all-gather.2.cloned.1.call-done, bf16[96,2048]{1,0:T(8,128)(2,1)S(1)} %copy-done.3), kind=kOutput, calls=%fused_computation.9 | convolution fusion | flops 403439520 | bytes 5570944 | tf_op jit(solution)/shard_map/dot_general | solution.py:407
  226.7 0.0 copy-done.5
  226.7 0.1 multiply_convert_fusion
  226.9 10.1 %all_gather.7 = bf16[192,2048]{1,0:T(8,128)(2,1)S(1)} all-gather(bf16[96,2048]{1,0:T(8,128)(2,1)S(1)} %multiply_convert_fusion), channel_id=1, replica_groups=mesh['sp'=16,'tp'=2] {'tp'}, dimensions={0}, use_global_device_ids=true | all-gather | bytes 1179648 | tf_op jit(solution)/shard_map/all_gather | solution.py:414
  237.0 8.0 %fusion.8 = f32[192,2816]{1,0:T(8,128)} fusion(bf16[192,2048]{1,0:T(8,128)(2,1)S(1)} %all_gather.7, bf16[2048,2816]{1,0:T(8,128)(2,1)} %get-tuple-element.14), kind=kOutput, calls=%fused_computation.35 | convolution fusion | flops 2214592512 | bytes 14483456 | tf_op jit(solution)/shard_map/dot_general | solution.py:415
  245.0 12.9 %fusion.2 = bf16[16,24,8,128]{3,2,1,0:T(8,128)(2,1)S(1)} fusion(bf16[16,2816,128]{2,1,0:T(8,128)(2,1)} %get-tuple-element.16, bf16[192,2048]{1,0:T(8,128)(2,1)S(1)} %all_gather.7, bf16[2048,2816]{1,0:T(8,128)(2,1)} %get-tuple-element.15, f32[192,2816]{1,0:T(8,128)} %fusion.8), kind=kOutput, calls=%fused_computation.5 | convolution fusion | flops 4432822272 | bytes 26804224 | tf_op jit(solution)/shard_map/th,nho->tno/dot_general | solution.py:418
  257.9 1.1 copy.42
  259.0 0.0 reduce-scatter.2.cloned.1.call-update
  259.0 17.4 %reduce-scatter.2.cloned.1.call-done = bf16[96,2048]{1,0:T(8,128)(2,1)} async-done(((bf16[192,2048]{1,0:T(8,128)(2,1)}), bf16[96,2048]{1,0:T(8,128)(2,1)}) %reduce-scatter.2.cloned.1.call-update) | async-done | bytes 393232 | tf_op jit(solution)/shard_map/reduce_scatter | solution.py:420
  276.5 1.8 add_convert_fusion
  (7 shorter events, 0.1 us)
Async XLA Ops:
  6.5 9.4 %copy-start.4 = (bf16[192,256]{1,0:T(8,128)(2,1)S(1)}, bf16[192,256]{1,0:T(8,128)(2,1)}, u32[]{:S(2)}) copy-start(bf16[192,256]{1,0:T(8,128)(2,1)} %param.13) | copy-start | bytes 294916
  6.5 10.3 %copy-start.2 = (bf16[2816,128]{1,0:T(8,128)(2,1)S(1)}, bf16[2816,128]{1,0:T(8,128)(2,1)}, u32[]{:S(2)}) copy-start(bf16[2816,128]{1,0:T(8,128)(2,1)} %wd_in.1) | copy-start | bytes 2162692
  6.5 10.3 %copy-start.1 = (bf16[128,2816]{1,0:T(8,128)(2,1)S(1)}, bf16[128,2816]{1,0:T(8,128)(2,1)}, u32[]{:S(2)}) copy-start(bf16[128,2816]{1,0:T(8,128)(2,1)} %wu_in.1) | copy-start | bytes 2162692
  6.5 10.3 %copy-start = (bf16[128,2816]{1,0:T(8,128)(2,1)S(1)}, bf16[128,2816]{1,0:T(8,128)(2,1)}, u32[]{:S(2)}) copy-start(bf16[128,2816]{1,0:T(8,128)(2,1)} %wg_in.1) | copy-start | bytes 2162692
  6.5 217.0 %all-gather.2.cloned.1.call-start = ((), (), s32[]{:S(2)}) async-start(), calls=%async_computation.2 | async-start | bytes 6291456 | tf_op jit(solution)/shard_map/all_gather | solution.py:408
  7.3 269.2 %reduce-scatter.2.cloned.1.call-start = ((), (), s32[]{:S(2)}) async-start(), calls=%async_computation.3 | async-start | bytes 1179648 | tf_op jit(solution)/shard_map/reduce_scatter | solution.py:420
  214.8 8.8 %copy-start.3 = (bf16[96,2048]{1,0:T(8,128)(2,1)S(1)}, bf16[96,2048]{1,0:T(8,128)(2,1)}, u32[]{:S(2)}) copy-start(bf16[96,2048]{1,0:T(8,128)(2,1)} %param.17) | copy-start | bytes 1179652
  215.6 11.1 %copy-start.5 = (f32[2048]{0:T(1024)S(1)}, f32[2048]{0:T(1024)}, u32[]{:S(2)}) copy-start(f32[2048]{0:T(1024)} %param.18) | copy-start | bytes 24580
Sparse Core Ops, SparseCore 0:
  8.9 58.6 all-gather.1
  259.2 17.2 reduce-scatter.1

commit v2 on v1

--- a/solution.py
+++ b/solution.py
@@ -142,7 +142,7 @@
         places = [(tuple(d.coords), d.core_on_chip) for d in mesh.devices[:, 0].flat]
     except AttributeError:
         return None
-    if count % 4 or count < 12:
+    if count % 4 or count < 12 or mesh.shape["tp"] != 2:
         return None
     first = places[0][0]
     depth = count // 4
@@ -180,11 +180,13 @@
     one(k_ref, kg_ref, k_out, 1.0)
 
 
-def gather_attend_kernel(
-    depth,
-    q_ref, kv_in, wg_in, wu_in, wd_in,
-    attn_ref, wg_out, wu_out, wd_out,
-    kv_all, own_sem, ring_send, ring_recv, sib_send, sib_recv,
+def layer_kernel(
+    depth, head_size,
+    q_ref, kv_in, wo_ref, res_ref, gain_ref, wg_in, wu_in, wd_in,
+    out_ref,
+    kv_all, wg_all, wu_all, wd_all, attn, partial, partial_in, mid, normed, hidden,
+    terms, kept, leaving, coming,
+    own_sem, ring_send, ring_recv, sib_send, sib_recv, x_send, x_recv,
 ):
     n = 2 * depth
     sp = lax.axis_index("sp")
@@ -201,39 +203,47 @@
         return (zz * 2 + yy) * 2 + c
 
     sibling = (at_pos(pos, 1 - core), tp)
+    partner = (sp, 1 - tp)
     toward = ((at_pos(pos + 1, core), tp), (at_pos(pos - 1, core), tp))
 
     barrier = pltpu.get_barrier_semaphore()
-    for target in (sibling,) + toward:
+    for target in (sibling, partner) + toward:
         pl.semaphore_signal(barrier, inc=1, device_id=target, device_id_type=MESH)
-    pl.semaphore_wait(barrier, 3)
+    pl.semaphore_wait(barrier, 4)
 
     tok = kv_in.shape[0]
     rows = wg_in.shape[0]
-
-    def half(size, way):
-        return pl.ds(way * (size // 2), size // 2)
+    units, lanes_down = wd_in.shape
+    KV, GATE, UP, LOW, HIGH = range(5)
+
+    def half(size, way, base=0):
+        return pl.ds(base + way * (size // 2), size // 2)
 
     def part(start, size, way):
         return pl.ds(pl.multiple_of(start * size + way * (size // 2), size // 2), size // 2)
+
+    def columns(o):
+        return pl.ds(pl.multiple_of(o * lanes_down, lanes_down), lanes_down)
 
     ins = (
         lambda way: kv_in.at[half(tok, way), :],
         lambda way: wg_in.at[half(rows, way), :],
         lambda way: wu_in.at[half(rows, way), :],
-        lambda way: wd_in.at[half(wd_in.shape[0], way), :],
+        lambda way: wd_in.at[half(units // 2, way), :],
+        lambda way: wd_in.at[half(units // 2, way, units // 2), :],
     )
     outs = (
         lambda o, way: kv_all.at[part(o, tok, way), :],
-        lambda o, way: wg_out.at[part(o, rows, way), :],
-        lambda o, way: wu_out.at[part(o, rows, way), :],
-        lambda o, way: wd_out.at[o, half(wd_in.shape[0], way), :],
+        lambda o, way: wg_all.at[part(o, rows, way), :],
+        lambda o, way: wu_all.at[part(o, rows, way), :],
+        lambda o, way: wd_all.at[half(units // 2, way), columns(o)],
+        lambda o, way: wd_all.at[half(units // 2, way, units // 2), columns(o)],
     )
     own_outs = (
         kv_all.at[pl.ds(pl.multiple_of(sp * tok, tok), tok), :],
-        wg_out.at[pl.ds(pl.multiple_of(sp * rows, rows), rows), :],
-        wu_out.at[pl.ds(pl.multiple_of(sp * rows, rows), rows), :],
-        wd_out.at[sp],
+        wg_all.at[pl.ds(pl.multiple_of(sp * rows, rows), rows), :],
+        wu_all.at[pl.ds(pl.multiple_of(sp * rows, rows), rows), :],
+        wd_all.at[:, columns(sp)],
     )
     own = [
         pltpu.make_async_copy(src, dst, own_sem.at[i])
@@ -243,30 +253,33 @@
     def owner(step, way, c):
         return at_pos(pos - step if way == 0 else pos + step, c)
 
+    def remote(src, dst, send_sem, recv_sem, target):
+        return pltpu.make_async_remote_copy(
+            src_ref=src, dst_ref=dst, send_sem=send_sem, recv_sem=recv_sem,
+            device_id=target, device_id_type=MESH,
+        )
+
     def ring(kind, step, way):
         o = owner(step, way, core)
         src = ins[kind](way) if step == 0 else outs[kind](o, way)
-        return pltpu.make_async_remote_copy(
-            src_ref=src, dst_ref=outs[kind](o, way),
-            send_sem=ring_send.at[kind, step, way], recv_sem=ring_recv.at[kind, step, way],
-            device_id=toward[way], device_id_type=MESH,
+        return remote(
+            src, outs[kind](o, way),
+            ring_send.at[kind, step, way], ring_recv.at[kind, step, way], toward[way],
         )
 
     def arrived(kind, step, way):
-        o = owner(step + 1, way, core)
-        pltpu.make_async_remote_copy(
-            src_ref=outs[kind](o, way), dst_ref=outs[kind](o, way),
-            send_sem=ring_send.at[kind, step, way], recv_sem=ring_recv.at[kind, step, way],
-            device_id=toward[way], device_id_type=MESH,
+        piece = outs[kind](owner(step + 1, way, core), way)
+        remote(
+            piece, piece,
+            ring_send.at[kind, step, way], ring_recv.at[kind, step, way], toward[way],
         ).wait_recv()
 
-    def across(kind, step, way, c):
-        o = owner(step, way, c)
+    def across(kind, step, way):
+        o = owner(step, way, core)
         src = ins[kind](way) if step == 0 else outs[kind](o, way)
-        return pltpu.make_async_remote_copy(
-            src_ref=src, dst_ref=outs[kind](o, way),
-            send_sem=sib_send.at[kind, step, way], recv_sem=sib_recv.at[kind, step, way],
-            device_id=sibling, device_id_type=MESH,
+        return remote(
+            src, outs[kind](o, way),
+            sib_send.at[kind, step, way], sib_recv.at[kind, step, way], sibling,
         )
 
     def serve(kind, step):
@@ -275,31 +288,16 @@
                 arrived(kind, step - 1, way)
             if step < n - 1:
                 ring(kind, step, way).start()
-            across(kind, step, way, core).start()
-
-    def finish(kind):
-        for step in range(n):
+            across(kind, step, way).start()
+
+    def sibling_gave(kind, steps):
+        for step in steps:
             for way in range(2):
-                if step < n - 1:
-                    ring(kind, step, way).wait_send()
-                across(kind, step, way, core).wait_send()
-                o = owner(step, way, 1 - core)
-                pltpu.make_async_remote_copy(
-                    src_ref=outs[kind](o, way), dst_ref=outs[kind](o, way),
-                    send_sem=sib_send.at[kind, step, way], recv_sem=sib_recv.at[kind, step, way],
-                    device_id=sibling, device_id_type=MESH,
+                piece = outs[kind](owner(step, way, 1 - core), way)
+                remote(
+                    piece, piece,
+                    sib_send.at[kind, step, way], sib_recv.at[kind, step, way], sibling,
                 ).wait_recv()
-
-    own[0].start()
-    for step in range(n):
-        serve(0, step)
-        if step == n - 2:
-            for kind in (1, 2, 3):
-                own[kind].start()
-    for kind in (1, 2, 3):
-        serve(kind, 0)
-    own[0].wait()
-    finish(0)
 
     pairs, q_rows, lanes = q_ref.shape
     block = math.gcd(q_rows, 256)
@@ -317,19 +315,156 @@
         weights = jnp.exp(scores - jnp.max(scores, axis=-1, keepdims=True))
         total = jnp.sum(weights, axis=-1, keepdims=True)
         mixed = jnp.dot(weights.astype(jnp.bfloat16), v, preferred_element_type=jnp.float32)
-        attn_ref[pair, span, :] = (mixed / total).astype(jnp.bfloat16)
-
-    todo = list(range(pairs * per_pair))
-    for step in range(1, n):
-        for kind in (1, 2, 3):
-            serve(kind, step)
-            if todo:
-                attend(todo.pop(0))
-    for at in todo:
-        attend(at)
-    for kind in (1, 2, 3):
-        own[kind].wait()
-        finish(kind)
+        attn[pair, span, :] = (mixed / total).astype(jnp.bfloat16)
+
+    width = wo_ref.shape[1]
+
+    def project():
+        group = q_rows // (2 * tok)
+        blocks = []
+        for pair in range(pairs):
+            for side in range(2):
+                for g in range(0, group, 2):
+                    lower = attn[pair, pl.ds((side * group + g) * tok, tok), :].astype(jnp.float32)
+                    upper = attn[pair, pl.ds((side * group + g + 1) * tok, tok), :].astype(jnp.float32)
+                    if side == 1:
+                        lower = pltpu.roll(lower, head_size, 1)
+                    else:
+                        upper = pltpu.roll(upper, head_size, 1)
+                    lane = lax.broadcasted_iota(jnp.int32, lower.shape, 1)
+                    blocks.append(jnp.where(lane < head_size, lower, upper).astype(jnp.bfloat16))
+        together = jnp.concatenate(blocks, axis=1)
+        wide = math.gcd(width, 512)
+        for at in range(0, width, wide):
+            partial[:, at:at + wide] = jnp.dot(
+                together, wo_ref[:, at:at + wide], preferred_element_type=jnp.float32
+            )
+
+    own_count = res_ref.shape[0]
+    mine = pl.ds(pl.multiple_of(tp * own_count, own_count), own_count)
+    theirs = pl.ds(pl.multiple_of((1 - tp) * own_count, own_count), own_count)
+    give_partial = remote(partial.at[theirs, :], partial_in, x_send.at[0], x_recv.at[0], partner)
+    give_normed = remote(
+        normed.at[mine, :], normed.at[mine, :], x_send.at[1], x_recv.at[1], partner
+    )
+    take_normed = remote(
+        normed.at[theirs, :], normed.at[theirs, :], x_send.at[1], x_recv.at[1], partner
+    )
+
+    def normalize():
+        give_partial.wait_recv()
+        value = res_ref[...].astype(jnp.float32) + (partial[mine, :] + partial_in[...])
+        mid[...] = value
+        scale = lax.rsqrt(jnp.mean(value * value, axis=-1, keepdims=True) + EPS)
+        normed[mine, :] = (value * scale * gain_ref[...]).astype(jnp.bfloat16)
+
+    tile = math.gcd(units, 256)
+
+    def feed(first, last):
+        @pl.loop(first, last)
+        def _(at):
+            cols = pl.ds(pl.multiple_of(at * tile, tile), tile)
+            x = normed[...]
+            gate = jnp.dot(x, wg_all[:, cols], preferred_element_type=jnp.float32)
+            up = jnp.dot(x, wu_all[:, cols], preferred_element_type=jnp.float32)
+            hidden[:, cols] = (gate / (1.0 + jnp.exp(-gate)) * up).astype(jnp.bfloat16)
+
+    def pair_columns(d):
+        o = at_pos(pos - d, 0)
+        return pl.ds(pl.multiple_of(o * lanes_down, 2 * lanes_down), 2 * lanes_down)
+
+    def give_terms(d):
+        return remote(leaving.at[d], coming.at[d], x_send.at[2 + d], x_recv.at[2 + d], partner)
+
+    def lower(d):
+        terms[...] = jnp.dot(
+            hidden[...], wd_all[:, pair_columns(d)], preferred_element_type=jnp.float32
+        )
+        kept[d] = terms[mine, :]
+        leaving[d] = terms[theirs, :].astype(jnp.bfloat16)
+
+    def emit(d):
+        give_terms(d).wait_recv()
+        cols = pair_columns(d)
+        down = kept[d] + coming[d].astype(jnp.float32)
+        out_ref[:, cols] = (mid[:, cols] + 0.5 * down).astype(jnp.bfloat16)
+
+    for copy in own:
+        copy.start()
+    early = [(kind, step) for step in range(n) for kind in (GATE, UP)]
+    blocks = pairs * per_pair
+    done_blocks = 0
+    for slot, (kind, step) in enumerate(early):
+        if slot < n:
+            serve(KV, slot)
+        serve(kind, step)
+        if slot == n:
+            own[KV].wait()
+            sibling_gave(KV, range(n))
+        if slot >= n:
+            target = min(blocks, -(-blocks * (slot - n + 1) // (n - 2)))
+            while done_blocks < target:
+                attend(done_blocks)
+                done_blocks += 1
+        if slot == 2 * n - 2:
+            project()
+        if slot == 2 * n - 1:
+            give_partial.start()
+    tiles = units // tile
+    fed = 0
+    feed_from, feed_slots = 3, n - 3
+    stage_of = {n // 2 + i: ([n // 2 - i, n // 2 + i] if i else [n // 2]) for i in range(n // 2)}
+    waiting = []
+    late = [(kind, step) for step in range(n) for kind in (LOW, HIGH)]
+    for slot, (kind, step) in enumerate(late):
+        serve(kind, step)
+        for d in waiting:
+            give_terms(d).start()
+        waiting = []
+        if slot == 0:
+            normalize()
+        if slot == 1:
+            give_normed.start()
+            for other in (GATE, UP):
+                own[other].wait()
+                sibling_gave(other, range(n))
+        if slot == feed_from - 1:
+            take_normed.wait_recv()
+        if feed_from - 1 <= slot < n:
+            target = min(tiles, -(-tiles * (slot - feed_from + 2) // (feed_slots + 1)))
+            if target > fed:
+                feed(fed, target)
+                fed = target
+        if slot == n:
+            own[3].wait()
+            for other in (LOW, HIGH):
+                sibling_gave(other, range(1))
+            lower(0)
+            waiting.append(0)
+        if kind == HIGH and step >= n // 2:
+            fresh = range(1, step + 1) if step == n // 2 else range(step, step + 1)
+            for other in (LOW, HIGH):
+                sibling_gave(other, fresh)
+            for d in stage_of[step]:
+                lower(d)
+                waiting.append(d)
+    give_terms(waiting[0]).start()
+    ready = [0] + [d for step in range(n // 2, n - 1) for d in stage_of[step]]
+    for d in ready:
+        emit(d)
+    give_terms(waiting[1]).start()
+    for d in waiting:
+        emit(d)
+    for kind in range(5):
+        for step in range(n):
+            for way in range(2):
+                if step < n - 1:
+                    ring(kind, step, way).wait_send()
+                across(kind, step, way).wait_send()
+    give_partial.wait_send()
+    give_normed.wait_send()
+    for d in range(n):
+        give_terms(d).wait_send()
 
 
 def fast_body(depth, queries, keys, values, q_gain, k_gain, w_out, residual, norm_gain, w_gate, w_up, w_down):
@@ -374,53 +509,43 @@
     any_space = pl.BlockSpec(memory_space=pl.ANY)
     vmem = pl.BlockSpec(memory_space=pltpu.VMEM)
     n = 2 * depth
-    attn_pad, wg_all, wu_all, wd_all = pl.pallas_call(
-        functools.partial(gather_attend_kernel, depth),
-        out_shape=(
-            jax.ShapeDtypeStruct(padded.shape, jnp.bfloat16),
-            jax.ShapeDtypeStruct((n_sp * w_gate.shape[0], w_gate.shape[1]), jnp.bfloat16),
-            jax.ShapeDtypeStruct((n_sp * w_up.shape[0], w_up.shape[1]), jnp.bfloat16),
-            jax.ShapeDtypeStruct((n_sp,) + w_down.shape, jnp.bfloat16),
-        ),
-        in_specs=[vmem, vmem, any_space, any_space, any_space],
-        out_specs=(vmem, any_space, any_space, any_space),
+    own_count, width = residual.shape
+    depth_in, units = w_gate.shape
+    lanes_down = w_down.shape[1]
+    bf16, f32 = jnp.bfloat16, jnp.float32
+    return pl.pallas_call(
+        functools.partial(layer_kernel, depth, head_size),
+        out_shape=jax.ShapeDtypeStruct(residual.shape, bf16),
+        in_specs=[vmem] * 5 + [any_space] * 3,
+        out_specs=vmem,
         scratch_shapes=[
-            pltpu.VMEM((tokens, kv.shape[1]), jnp.bfloat16),
+            pltpu.VMEM((tokens, kv.shape[1]), bf16),
+            pltpu.VMEM((n_sp * depth_in, units), bf16),
+            pltpu.VMEM((n_sp * depth_in, units), bf16),
+            pltpu.VMEM((units, n_sp * lanes_down), bf16),
+            pltpu.VMEM(padded.shape, bf16),
+            pltpu.VMEM((tok_rows, width), f32),
+            pltpu.VMEM((own_count, width), f32),
+            pltpu.VMEM((own_count, width), f32),
+            pltpu.VMEM((tok_rows, width), bf16),
+            pltpu.VMEM((tok_rows, units), bf16),
+            pltpu.VMEM((tok_rows, 2 * lanes_down), f32),
+            pltpu.VMEM((n, own_count, 2 * lanes_down), f32),
+            pltpu.VMEM((n, own_count, 2 * lanes_down), bf16),
+            pltpu.VMEM((n, own_count, 2 * lanes_down), bf16),
             pltpu.SemaphoreType.DMA((4,)),
-            pltpu.SemaphoreType.DMA((4, n - 1, 2)),
-            pltpu.SemaphoreType.DMA((4, n - 1, 2)),
-            pltpu.SemaphoreType.DMA((4, n, 2)),
-            pltpu.SemaphoreType.DMA((4, n, 2)),
+            pltpu.SemaphoreType.DMA((5, n - 1, 2)),
+            pltpu.SemaphoreType.DMA((5, n - 1, 2)),
+            pltpu.SemaphoreType.DMA((5, n, 2)),
+            pltpu.SemaphoreType.DMA((5, n, 2)),
+            pltpu.SemaphoreType.DMA((2 + n,)),
+            pltpu.SemaphoreType.DMA((2 + n,)),
         ],
         compiler_params=pltpu.CompilerParams(
-            collective_id=0, has_side_effects=True, vmem_limit_bytes=48 * 1024 * 1024
+            collective_id=0, has_side_effects=True, vmem_limit_bytes=63 * 1024 * 1024
         ),
-        cost_estimate=pl.CostEstimate(
-            flops=150_000_000_000, bytes_accessed=80_000_000, transcendentals=0
-        ),
-        name="gather_attend",
-    )(padded, kv, w_gate, w_up, w_down)
-    parts = attn_pad.reshape(pairs, 2, q_group, tok_rows, 2, head_size)
-    attn = jnp.stack([parts[:, 0, :, :, 0], parts[:, 1, :, :, 1]], axis=1)
-    attn = jnp.transpose(attn, (3, 0, 1, 2, 4)).reshape(tok_rows, q_heads * head_size)
-    own_rows = lax.all_to_all(attn, "tp", split_axis=0, concat_axis=1, tiled=True)
-    proj = jnp.dot(
-        own_rows, lax.all_gather(w_out, "tp", axis=0, tiled=True), preferred_element_type=jnp.float32
-    )
-    mid = residual.astype(jnp.float32) + proj
-    normed = (
-        mid * lax.rsqrt(jnp.mean(mid * mid, axis=-1, keepdims=True) + EPS) * norm_gain
-    ).astype(jnp.bfloat16)
-    columns = lax.all_gather(normed, "tp", axis=0, tiled=True)
-    gate = jnp.dot(columns, wg_all, preferred_element_type=jnp.float32)
-    up_part = jnp.dot(columns, wu_all, preferred_element_type=jnp.float32)
-    hidden = (jax.nn.silu(gate) * up_part).astype(jnp.bfloat16)
-    terms = jnp.einsum("th,nho->tno", hidden, wd_all, preferred_element_type=jnp.float32)
-    terms = terms.reshape(tok_rows, -1)
-    down = lax.psum_scatter(
-        terms.astype(jnp.bfloat16), "tp", scatter_dimension=0, tiled=True
-    ).astype(jnp.float32)
-    return (mid + 0.5 * down).astype(jnp.bfloat16)
+        name="layer",
+    )(padded, kv, w_out, residual, norm_gain[None, :], w_gate, w_up, w_down)
 
 
 def solution(mesh):

time: 286 us -> 222 us (0.78)
  matrix products: 24 us -> 0 us
  waiting for transfers between devices: 18.2 us -> 0 us
  blocking collectives: 16.8 us -> 0 us
  between operations: 13.6 us -> 0.07 us
  Pallas kernels: 201 us -> 213 us
    dot_general x3 -> x0, matrix products: 24 us -> none  [the longest x1 12.9 us: fast_body(): jnp.einsum('th,nho->tno', hidden, wd_all, preferred_element_type=jnp.floa...]
    reduce_scatter x1 -> x0, waiting for transfers between devices: 17.4 us -> none  [fast_body(): lax.psum_scatter(terms.astype(jnp.bfloat16), 'tp', scatter_dimension=0, t...]
    pallas_call x1, Pallas kernels: 198 us -> 210 us  [fast_body(): pl.pallas_call(functools.partial(layer_kernel, depth, head_size), out_sha...]
    all_gather x1 -> x0, blocking collectives: 10.1 us -> none  [fast_body(): columns = lax.all_gather(normed, 'tp', axis=0, tiled=True)]
    all_to_all x1 -> x0, blocking collectives: 6.69 us -> none  [fast_body(): lax.all_to_all(attn, 'tp', split_axis=0, concat_axis=1, tiled=True)]
  transfers between devices with their start and end apart: 2 -> 0, of which waited for: 1 -> 0; matrix products, arithmetic and copies ran while one was open for 3% -> 0% of each run, Pallas kernels for 70% -> 0%
where the time goes in v2:
time: 222 us
  Pallas kernels  213 us (96%)
  local copies, waits for them, and re-layouts  7.79 us (4%)
    pallas_call x1, Pallas kernels, fast_body(): pl.pallas_call(functools.partial(layer_kernel, depth, head_size), out_sha...  210 us

profile of v2, /device:TPU:1, one launch (start us, length us, event | category | flops | bytes accessed | tf_op | source)
XLA Modules:
  0.0 221.8 jit_solution(7280336793400987945)
XLA Ops:
  0.0 0.1 broadcast_multiply_fusion
  0.2 0.3 concatenate.12
  0.4 1.0 fusion.3
  1.4 0.7 tile.4
  2.1 0.6 broadcast_in_dim_tile.6.qg_ref
  2.7 0.7 tile.5
  3.4 0.7 broadcast_in_dim_tile.7.kg_ref
  4.1 0.0 copy-start
  4.1 3.0 %rope.1 = (bf16[192,512]{1,0:T(8,128)(2,1)}, bf16[192,256]{1,0:T(8,128)(2,1)}) custom-call(bf16[192,512]{1,0:T(8,128)(2,1)} %q_ref.1, bf16[192,256]{1,0:T(8,128)(2,1)} %k_ref.1, f32[1,512]{1,0:T(1,128)} %broadcast_in_dim_tile.6.qg_ref, f32[1,256]{1,0:T(1,128)} %broadcast_in_dim_tile.7.kg_ref, f32[192,128]{1,0:T(8,128)} %get-tuple-element.12.cos_ref, ...), custom_call_target="tpu_custom_call" | custom-call | tf_op jit(solution)/shard_map/rope/pallas_call | solution.py:484
  7.1 0.0 copy-start.1
  7.1 1.1 copy.14
  8.3 0.1 pad_maximum_fusion
  8.4 1.0 copy.16
  9.3 0.0 copy-done
  9.3 0.0 copy-done.1
  9.3 0.7 pad_maximum_fusion.1.kv_in
  10.0 210.0 %layer.1 = bf16[96,2048]{1,0:T(8,128)(2,1)} custom-call(bf16[2,768,128]{2,1,0:T(8,128)(2,1)} %bitcast.15, bf16[192,512]{1,0:T(8,128)(2,1)} %pad_maximum_fusion.1.kv_in, bf16[512,2048]{1,0:T(8,128)(2,1)} %wo_ref.1, bf16[96,2048]{1,0:T(8,128)(2,1)} %res_ref.1, f32[1,2048]{1,0:T(1,128)} %bitcast.17, bf16[128,2816]{1,0:T(8,128)(2,1)} %wg_in.1, ...), custom_call_target="tpu_custom_call" | custom-call | tf_op jit(solution)/shard_map/layer/pallas_call | solution.py:516
  220.0 1.8 copy.19
  (5 shorter events, 0.1 us)
Async XLA Ops:
  4.1 5.3 %copy-start = (bf16[192,256]{1,0:T(8,128)(2,1)S(1)}, bf16[192,256]{1,0:T(8,128)(2,1)}, u32[]{:S(2)}) copy-start(bf16[192,256]{1,0:T(8,128)(2,1)} %param.13) | copy-start | bytes 294916
  7.1 2.3 %copy-start.1 = (bf16[192,256]{1,0:T(8,128)(2,1)S(1)}, bf16[192,256]{1,0:T(8,128)(2,1)}, u32[]{:S(2)}) copy-start(bf16[192,256]{1,0:T(8,128)(2,1)} %get-tuple-element.8) | copy-start | bytes 294916

commit v3 on v2

--- a/solution.py
+++ b/solution.py
@@ -164,7 +164,7 @@
         mean = jnp.dot(
             x * x, same, preferred_element_type=jnp.float32, precision=lax.Precision.HIGHEST
         ) * (1.0 / head_size)
-        h = x * lax.rsqrt(mean + EPS) * g_ref[...]
+        h = x * lax.rsqrt(mean + EPS) * jnp.concatenate([g_ref[...]] * (width // head_size), axis=1)
         quarter = head_size // 4
         repeats = width // cos_ref.shape[1]
         cos_table = jnp.concatenate([cos_ref[...]] * repeats, axis=1)
@@ -182,9 +182,9 @@
 
 def layer_kernel(
     depth, head_size,
-    q_ref, kv_in, wo_ref, res_ref, gain_ref, wg_in, wu_in, wd_in,
+    q_ref, kv_in, res_ref, gain_ref, wo_in, wg_in, wu_in, wd_in,
     out_ref,
-    kv_all, wg_all, wu_all, wd_all, attn, partial, partial_in, mid, normed, hidden,
+    kv_all, wg_all, wu_all, wd_all, wo_own, wo_other, attn, context, context_in, mid, normed, hidden,
     terms, kept, leaving, coming,
     own_sem, ring_send, ring_recv, sib_send, sib_recv, x_send, x_recv,
 ):
@@ -244,10 +244,11 @@
         wg_all.at[pl.ds(pl.multiple_of(sp * rows, rows), rows), :],
         wu_all.at[pl.ds(pl.multiple_of(sp * rows, rows), rows), :],
         wd_all.at[:, columns(sp)],
+        wo_own,
     )
     own = [
         pltpu.make_async_copy(src, dst, own_sem.at[i])
-        for i, (src, dst) in enumerate(zip((kv_in, wg_in, wu_in, wd_in), own_outs))
+        for i, (src, dst) in enumerate(zip((kv_in, wg_in, wu_in, wd_in, wo_in), own_outs))
     ]
 
     def owner(step, way, c):
@@ -317,9 +318,9 @@
         mixed = jnp.dot(weights.astype(jnp.bfloat16), v, preferred_element_type=jnp.float32)
         attn[pair, span, :] = (mixed / total).astype(jnp.bfloat16)
 
-    width = wo_ref.shape[1]
-
-    def project():
+    width = wo_in.shape[1]
+
+    def assemble():
         group = q_rows // (2 * tok)
         blocks = []
         for pair in range(pairs):
@@ -333,17 +334,13 @@
                         upper = pltpu.roll(upper, head_size, 1)
                     lane = lax.broadcasted_iota(jnp.int32, lower.shape, 1)
                     blocks.append(jnp.where(lane < head_size, lower, upper).astype(jnp.bfloat16))
-        together = jnp.concatenate(blocks, axis=1)
-        wide = math.gcd(width, 512)
-        for at in range(0, width, wide):
-            partial[:, at:at + wide] = jnp.dot(
-                together, wo_ref[:, at:at + wide], preferred_element_type=jnp.float32
-            )
+        context[...] = jnp.concatenate(blocks, axis=1)
 
     own_count = res_ref.shape[0]
     mine = pl.ds(pl.multiple_of(tp * own_count, own_count), own_count)
     theirs = pl.ds(pl.multiple_of((1 - tp) * own_count, own_count), own_count)
-    give_partial = remote(partial.at[theirs, :], partial_in, x_send.at[0], x_recv.at[0], partner)
+    give_context = remote(context.at[theirs, :], context_in, x_send.at[0], x_recv.at[0], partner)
+    give_wo = remote(wo_in, wo_other, x_send.at[2 + n], x_recv.at[2 + n], partner)
     give_normed = remote(
         normed.at[mine, :], normed.at[mine, :], x_send.at[1], x_recv.at[1], partner
     )
@@ -352,9 +349,18 @@
     )
 
     def normalize():
-        give_partial.wait_recv()
-        value = res_ref[...].astype(jnp.float32) + (partial[mine, :] + partial_in[...])
-        mid[...] = value
+        give_context.wait_recv()
+        give_wo.wait_recv()
+        own[4].wait()
+        held, other = context[mine, :], context_in[...]
+        wide = math.gcd(width, 512)
+        for at in range(0, width, wide):
+            cols = slice(at, at + wide)
+            mid[:, cols] = res_ref[:, cols].astype(jnp.float32) + (
+                jnp.dot(held, wo_own[:, cols], preferred_element_type=jnp.float32)
+                + jnp.dot(other, wo_other[:, cols], preferred_element_type=jnp.float32)
+            )
+        value = mid[...]
         scale = lax.rsqrt(jnp.mean(value * value, axis=-1, keepdims=True) + EPS)
         normed[mine, :] = (value * scale * gain_ref[...]).astype(jnp.bfloat16)
 
@@ -398,6 +404,11 @@
         if slot < n:
             serve(KV, slot)
         serve(kind, step)
+        if slot == 1:
+            give_wo.start()
+        if slot == 2 * n - 3:
+            for ahead in (LOW, HIGH):
+                serve(ahead, 0)
         if slot == n:
             own[KV].wait()
             sibling_gave(KV, range(n))
@@ -406,24 +417,25 @@
             while done_blocks < target:
                 attend(done_blocks)
                 done_blocks += 1
+        if slot == 2 * n - 3:
+            assemble()
         if slot == 2 * n - 2:
-            project()
+            give_context.start()
         if slot == 2 * n - 1:
-            give_partial.start()
+            normalize()
     tiles = units // tile
     fed = 0
-    feed_from, feed_slots = 3, n - 3
+    feed_from, feed_slots = 5, n - 5
     stage_of = {n // 2 + i: ([n // 2 - i, n // 2 + i] if i else [n // 2]) for i in range(n // 2)}
     waiting = []
     late = [(kind, step) for step in range(n) for kind in (LOW, HIGH)]
     for slot, (kind, step) in enumerate(late):
-        serve(kind, step)
+        if step > 0:
+            serve(kind, step)
         for d in waiting:
             give_terms(d).start()
         waiting = []
-        if slot == 0:
-            normalize()
-        if slot == 1:
+        if slot == 2:
             give_normed.start()
             for other in (GATE, UP):
                 own[other].wait()
@@ -461,7 +473,8 @@
                 if step < n - 1:
                     ring(kind, step, way).wait_send()
                 across(kind, step, way).wait_send()
-    give_partial.wait_send()
+    give_context.wait_send()
+    give_wo.wait_send()
     give_normed.wait_send()
     for d in range(n):
         give_terms(d).wait_send()
@@ -490,7 +503,7 @@
         name="rope",
     )(
         queries, keys,
-        jnp.tile(q_gain, q_heads)[None, :], jnp.tile(k_gain, kv_heads)[None, :],
+        q_gain[None, :], k_gain[None, :],
         cos_table, sin_table,
     )
     pairs = kv_heads // 2
@@ -516,16 +529,18 @@
     return pl.pallas_call(
         functools.partial(layer_kernel, depth, head_size),
         out_shape=jax.ShapeDtypeStruct(residual.shape, bf16),
-        in_specs=[vmem] * 5 + [any_space] * 3,
+        in_specs=[vmem] * 4 + [any_space] * 4,
         out_specs=vmem,
         scratch_shapes=[
             pltpu.VMEM((tokens, kv.shape[1]), bf16),
             pltpu.VMEM((n_sp * depth_in, units), bf16),
             pltpu.VMEM((n_sp * depth_in, units), bf16),
             pltpu.VMEM((units, n_sp * lanes_down), bf16),
+            pltpu.VMEM(w_out.shape, bf16),
+            pltpu.VMEM(w_out.shape, bf16),
             pltpu.VMEM(padded.shape, bf16),
-            pltpu.VMEM((tok_rows, width), f32),
-            pltpu.VMEM((own_count, width), f32),
+            pltpu.VMEM(queries.shape, bf16),
+            pltpu.VMEM((own_count, queries.shape[1]), bf16),
             pltpu.VMEM((own_count, width), f32),
             pltpu.VMEM((tok_rows, width), bf16),
             pltpu.VMEM((tok_rows, units), bf16),
@@ -533,19 +548,19 @@
             pltpu.VMEM((n, own_count, 2 * lanes_down), f32),
             pltpu.VMEM((n, own_count, 2 * lanes_down), bf16),
             pltpu.VMEM((n, own_count, 2 * lanes_down), bf16),
-            pltpu.SemaphoreType.DMA((4,)),
+            pltpu.SemaphoreType.DMA((5,)),
             pltpu.SemaphoreType.DMA((5, n - 1, 2)),
             pltpu.SemaphoreType.DMA((5, n - 1, 2)),
             pltpu.SemaphoreType.DMA((5, n, 2)),
             pltpu.SemaphoreType.DMA((5, n, 2)),
-            pltpu.SemaphoreType.DMA((2 + n,)),
-            pltpu.SemaphoreType.DMA((2 + n,)),
+            pltpu.SemaphoreType.DMA((3 + n,)),
+            pltpu.SemaphoreType.DMA((3 + n,)),
         ],
         compiler_params=pltpu.CompilerParams(
             collective_id=0, has_side_effects=True, vmem_limit_bytes=63 * 1024 * 1024
         ),
         name="layer",
-    )(padded, kv, w_out, residual, norm_gain[None, :], w_gate, w_up, w_down)
+    )(padded, kv, residual, norm_gain[None, :], w_out, w_gate, w_up, w_down)
 
 
 def solution(mesh):

time: 222 us -> 202 us (0.910)
  Pallas kernels: 213 us -> 196 us
  local copies, waits for them, and re-layouts: 7.79 us -> 5.16 us
    pallas_call x1, Pallas kernels: 210 us -> 193 us  [fast_body(): pl.pallas_call(functools.partial(layer_kernel, depth, head_size), out_sha...]
    another operation x4 -> x0, local copies, waits for them, and re-layouts: 2.62 us -> none  [the longest x2 1.33 us: fast_body(): jnp.tile(k_gain, kv_heads)[None, :]]
where the time goes in v3:
time: 202 us
  Pallas kernels  196 us (97%)
  local copies, waits for them, and re-layouts  5.16 us (3%)
    pallas_call x1, Pallas kernels, fast_body(): pl.pallas_call(functools.partial(layer_kernel, depth, head_size), out_sha...  193 us

profile of v3, /device:TPU:1, one launch (start us, length us, event | category | flops | bytes accessed | tf_op | source)
XLA Modules:
  0.0 202.0 jit_solution(2624020405088816973)
XLA Ops:
  0.0 0.1 broadcast_multiply_fusion
  0.2 0.3 concatenate.12
  0.4 1.0 fusion.3
  1.4 0.0 copy-start
  1.4 3.0 %rope.1 = (bf16[192,512]{1,0:T(8,128)(2,1)}, bf16[192,256]{1,0:T(8,128)(2,1)}) custom-call(bf16[192,512]{1,0:T(8,128)(2,1)} %q_ref.1, bf16[192,256]{1,0:T(8,128)(2,1)} %k_ref.1, f32[1,64]{1,0:T(1,128)} %bitcast.20, f32[1,64]{1,0:T(1,128)} %bitcast.21, f32[192,128]{1,0:T(8,128)} %get-tuple-element.12.cos_ref, f32[192,128]{1,0:T(8,128)} %get-tuple-element.11.sin_ref), custom_call_target="tpu_custom_call" | custom-call | tf_op jit(solution)/shard_map/rope/pallas_call | solution.py:497
  4.5 0.0 copy-start.1
  4.5 1.1 copy.14
  5.7 0.1 pad_maximum_fusion
  5.8 1.0 copy.16
  6.7 0.0 copy-done
  6.7 0.0 copy-done.1
  6.7 0.7 pad_maximum_fusion.1.kv_in
  7.4 192.8 %layer.1 = bf16[96,2048]{1,0:T(8,128)(2,1)} custom-call(bf16[2,768,128]{2,1,0:T(8,128)(2,1)} %bitcast.17, bf16[192,512]{1,0:T(8,128)(2,1)} %pad_maximum_fusion.1.kv_in, bf16[96,2048]{1,0:T(8,128)(2,1)} %res_ref.1, f32[1,2048]{1,0:T(1,128)} %bitcast.19, bf16[512,2048]{1,0:T(8,128)(2,1)} %wo_in.1, bf16[128,2816]{1,0:T(8,128)(2,1)} %wg_in.1, ...), custom_call_target="tpu_custom_call" | custom-call | tf_op jit(solution)/shard_map/layer/pallas_call | solution.py:529
  200.2 1.8 copy.19
  (5 shorter events, 0.1 us)
Async XLA Ops:
  1.4 5.3 %copy-start = (bf16[192,256]{1,0:T(8,128)(2,1)S(1)}, bf16[192,256]{1,0:T(8,128)(2,1)}, u32[]{:S(2)}) copy-start(bf16[192,256]{1,0:T(8,128)(2,1)} %param.13) | copy-start | bytes 294916
  4.5 2.3 %copy-start.1 = (bf16[192,256]{1,0:T(8,128)(2,1)S(1)}, bf16[192,256]{1,0:T(8,128)(2,1)}, u32[]{:S(2)}) copy-start(bf16[192,256]{1,0:T(8,128)(2,1)} %get-tuple-element.8) | copy-start | bytes 294916

commit v4 on v3

--- a/solution.py
+++ b/solution.py
@@ -154,37 +154,33 @@
     return depth
 
 
-def rope_kernel(head_size, q_ref, k_ref, qg_ref, kg_ref, cos_ref, sin_ref, q_out, k_out):
-    def one(x_ref, g_ref, out_ref, scale):
-        x = x_ref[...].astype(jnp.float32)
-        width = x.shape[1]
-        lane = lax.broadcasted_iota(jnp.int32, (width, width), 0) // head_size
-        other = lax.broadcasted_iota(jnp.int32, (width, width), 1) // head_size
-        same = (lane == other).astype(jnp.float32)
-        mean = jnp.dot(
-            x * x, same, preferred_element_type=jnp.float32, precision=lax.Precision.HIGHEST
-        ) * (1.0 / head_size)
-        h = x * lax.rsqrt(mean + EPS) * jnp.concatenate([g_ref[...]] * (width // head_size), axis=1)
-        quarter = head_size // 4
-        repeats = width // cos_ref.shape[1]
-        cos_table = jnp.concatenate([cos_ref[...]] * repeats, axis=1)
-        sin_table = jnp.concatenate([sin_ref[...]] * repeats, axis=1)
-        at = lax.broadcasted_iota(jnp.int32, x.shape, 1)
-        is_first = (at // quarter) % 2 == 0
-        ahead = pltpu.roll(h, width - quarter, 1)
-        behind = pltpu.roll(h, quarter, 1)
-        turned = h * cos_table + jnp.where(is_first, -ahead, behind) * sin_table
-        out_ref[...] = (turned.astype(jnp.bfloat16) * scale).astype(jnp.bfloat16)
-
-    one(q_ref, qg_ref, q_out, head_size ** (-0.5))
-    one(k_ref, kg_ref, k_out, 1.0)
+def turned_heads(head_size, x_ref, g_ref, cos_ref, sin_ref):
+    x = x_ref[...].astype(jnp.float32)
+    width = x.shape[1]
+    lane = lax.broadcasted_iota(jnp.int32, (width, width), 0) // head_size
+    other = lax.broadcasted_iota(jnp.int32, (width, width), 1) // head_size
+    same = (lane == other).astype(jnp.float32)
+    mean = jnp.dot(
+        x * x, same, preferred_element_type=jnp.float32, precision=lax.Precision.HIGHEST
+    ) * (1.0 / head_size)
+    h = x * lax.rsqrt(mean + EPS) * jnp.concatenate([g_ref[...]] * (width // head_size), axis=1)
+    quarter = head_size // 4
+    repeats = width // cos_ref.shape[1]
+    cos_table = jnp.concatenate([cos_ref[...]] * repeats, axis=1)
+    sin_table = jnp.concatenate([sin_ref[...]] * repeats, axis=1)
+    at = lax.broadcasted_iota(jnp.int32, x.shape, 1)
+    is_first = (at // quarter) % 2 == 0
+    ahead = pltpu.roll(h, width - quarter, 1)
+    behind = pltpu.roll(h, quarter, 1)
+    turned = h * cos_table + jnp.where(is_first, -ahead, behind) * sin_table
+    return turned.astype(jnp.bfloat16)
 
 
 def layer_kernel(
     depth, head_size,
-    q_ref, kv_in, res_ref, gain_ref, wo_in, wg_in, wu_in, wd_in,
+    raw_q, raw_k, raw_v, qg_ref, kg_ref, cos_ref, sin_ref, res_ref, gain_ref, wo_in, wg_in, wu_in, wd_in,
     out_ref,
-    kv_all, wg_all, wu_all, wd_all, wo_own, wo_other, attn, context, context_in, mid, normed, hidden,
+    q_ref, kv_in, kv_all, wg_all, wu_all, wd_all, wo_own, wo_other, attn, context, context_in, mid, normed, hidden,
     terms, kept, leaving, coming,
     own_sem, ring_send, ring_recv, sib_send, sib_recv, x_send, x_recv,
 ):
@@ -395,15 +391,35 @@
         down = kept[d] + coming[d].astype(jnp.float32)
         out_ref[:, cols] = (mid[:, cols] + 0.5 * down).astype(jnp.bfloat16)
 
-    for copy in own:
+    for copy in own[1:]:
         copy.start()
+    serve(GATE, 0)
+    k_width = raw_k.shape[1]
+    kv_in[:, :k_width] = turned_heads(head_size, raw_k, kg_ref, cos_ref, sin_ref)
+    kv_in[:, k_width:] = raw_v[...]
+    turned = turned_heads(head_size, raw_q, qg_ref, cos_ref, sin_ref).astype(jnp.float32)
+    turned = turned * head_size ** (-0.5)
+    group = q_rows // (2 * tok)
+    for at in range(raw_q.shape[1] // lanes):
+        both = turned[:, at * lanes:(at + 1) * lanes]
+        swapped = pltpu.roll(both, head_size, 1)
+        low = lax.broadcasted_iota(jnp.int32, both.shape, 1) < head_size
+        key_head, g = 2 * at // group, 2 * at % group
+        pair, side = key_head // 2, key_head % 2
+        for extra in range(2):
+            source = both if extra == side else swapped
+            kept_lanes = jnp.where(low if side == 0 else jnp.logical_not(low), source, 0.0)
+            first = (side * group + g + extra) * tok
+            q_ref[pair, first:first + tok, :] = kept_lanes.astype(jnp.bfloat16)
+    own[KV].start()
     early = [(kind, step) for step in range(n) for kind in (GATE, UP)]
     blocks = pairs * per_pair
     done_blocks = 0
     for slot, (kind, step) in enumerate(early):
         if slot < n:
             serve(KV, slot)
-        serve(kind, step)
+        if slot > 0:
+            serve(kind, step)
         if slot == 1:
             give_wo.start()
         if slot == 2 * n - 3:
@@ -494,30 +510,9 @@
     col_angle = (positions % GRID_W).astype(jnp.float32)[:, None] * inv_freq[None, :]
     angle = jnp.concatenate([row_angle, row_angle, col_angle, col_angle] * 2, axis=1)
     cos_table, sin_table = jnp.cos(angle), jnp.sin(angle)
-    q_rot, k_rot = pl.pallas_call(
-        functools.partial(rope_kernel, head_size),
-        out_shape=(
-            jax.ShapeDtypeStruct(queries.shape, jnp.bfloat16),
-            jax.ShapeDtypeStruct(keys.shape, jnp.bfloat16),
-        ),
-        name="rope",
-    )(
-        queries, keys,
-        q_gain[None, :], k_gain[None, :],
-        cos_table, sin_table,
-    )
     pairs = kv_heads // 2
-    grouped = q_rot.reshape(tok_rows, pairs, 2, q_group, head_size)
-    grouped = jnp.transpose(grouped, (1, 2, 3, 0, 4))
-    empty = jnp.zeros_like(grouped[:, 0])
-    padded = jnp.stack(
-        [
-            jnp.concatenate([grouped[:, 0], empty], axis=-1),
-            jnp.concatenate([empty, grouped[:, 1]], axis=-1),
-        ],
-        axis=1,
-    ).reshape(pairs, 2 * q_group * tok_rows, 2 * head_size)
-    kv = jnp.concatenate([k_rot, values], axis=1)
+    padded = (pairs, 2 * q_group * tok_rows, 2 * head_size)
+    kv_shape = (tok_rows, keys.shape[1] + values.shape[1])
     tokens = n_sp * tok_rows
     any_space = pl.BlockSpec(memory_space=pl.ANY)
     vmem = pl.BlockSpec(memory_space=pltpu.VMEM)
@@ -529,16 +524,18 @@
     return pl.pallas_call(
         functools.partial(layer_kernel, depth, head_size),
         out_shape=jax.ShapeDtypeStruct(residual.shape, bf16),
-        in_specs=[vmem] * 4 + [any_space] * 4,
+        in_specs=[vmem] * 9 + [any_space] * 4,
         out_specs=vmem,
         scratch_shapes=[
-            pltpu.VMEM((tokens, kv.shape[1]), bf16),
+            pltpu.VMEM(padded, bf16),
+            pltpu.VMEM(kv_shape, bf16),
+            pltpu.VMEM((tokens, kv_shape[1]), bf16),
             pltpu.VMEM((n_sp * depth_in, units), bf16),
             pltpu.VMEM((n_sp * depth_in, units), bf16),
             pltpu.VMEM((units, n_sp * lanes_down), bf16),
             pltpu.VMEM(w_out.shape, bf16),
             pltpu.VMEM(w_out.shape, bf16),
-            pltpu.VMEM(padded.shape, bf16),
+            pltpu.VMEM(padded, bf16),
             pltpu.VMEM(queries.shape, bf16),
             pltpu.VMEM((own_count, queries.shape[1]), bf16),
             pltpu.VMEM((own_count, width), f32),
@@ -560,7 +557,9 @@
             collective_id=0, has_side_effects=True, vmem_limit_bytes=63 * 1024 * 1024
         ),
         name="layer",
-    )(padded, kv, residual, norm_gain[None, :], w_out, w_gate, w_up, w_down)
+    )(
+        queries, keys, values, q_gain[None, :], k_gain[None, :], cos_table, sin_table,
+        residual, norm_gain[None, :], w_out, w_gate, w_up, w_down)
 
 
 def solution(mesh):

time: 202 us -> 198 us (0.980)
  local copies, waits for them, and re-layouts: 5.16 us -> 3.04 us
    pallas_call x1 -> x0, Pallas kernels: 3.04 us -> none  [fast_body(): pl.pallas_call(functools.partial(rope_kernel, head_size), out_shape=(jax....]
where the time goes in v4:
time: 198 us; the launch traced here: 197 us
  Pallas kernels  194 us (98%)
  local copies, waits for them, and re-layouts  3.04 us (2%)
    pallas_call x1, Pallas kernels, fast_body(): pl.pallas_call(functools.partial(layer_kernel, depth, head_size), out_sha...  194 us

profile of v4, /device:TPU:1, one launch (start us, length us, event | category | flops | bytes accessed | tf_op | source)
XLA Modules:
  0.0 197.5 jit_solution(5867320484518702156)
XLA Ops:
  0.0 0.1 broadcast_multiply_fusion
  0.2 0.3 concatenate.3
  0.4 1.0 fusion.3
  1.4 194.3 %layer.1 = bf16[96,2048]{1,0:T(8,128)(2,1)} custom-call(bf16[192,512]{1,0:T(8,128)(2,1)} %raw_q.1, bf16[192,256]{1,0:T(8,128)(2,1)} %raw_k.1, bf16[192,256]{1,0:T(8,128)(2,1)} %raw_v.1, f32[1,64]{1,0:T(1,128)} %bitcast.4, f32[1,64]{1,0:T(1,128)} %bitcast.5, f32[192,128]{1,0:T(8,128)} %get-tuple-element.6.cos_ref, f32[192,128]{1,0:T(8,128)} %get-tuple-element.5.sin_ref, ...), custom_call_target="tpu_custom_call" | custom-call | tf_op jit(solution)/shard_map/layer/pallas_call | solution.py:524
  195.7 1.8 copy.13
  (2 shorter events, 0.0 us)
